TPU v7x, 512 devices: a whole 4x8x8 slice. The times are simulated.
512 devices in a mesh: ep: 32 (over z, x), tp: 16 (over y, core).
Axes of the slice: x: 4, y: 8, z: 8, core: 2. Of those that a mesh axis runs over, the one named last changes fastest.
Arguments:
- tokens: bfloat16 [8192, 2048], P('ep')
- norm_gain: float32 [2048], replicated, may hold values from 0.1 to 1.9
- chosen: int32 [32, 1024], replicated, may hold values from 0 to 8191, as said below
- route_weight: float32 [32, 1024], P('ep'), may hold values from 0.2 to 1
- gate_weight: bfloat16 [32, 2048, 4096], P('ep', None, 'tp'), may hold values from -0.125 to 0.125
- up_weight: bfloat16 [32, 2048, 4096], P('ep', None, 'tp'), may hold values from -0.125 to 0.125
- down_weight: bfloat16 [32, 4096, 2048], P('ep', 'tp'), may hold values from -0.09375 to 0.09375
Outputs:
- combined: bfloat16 [8192, 2048], P('ep', 'tp')
Inputs may be any that keep to these rules, and one draw needn't show every extreme that they name: Each row of chosen lists 1024 distinct token numbers in ascending order. Of the 256 consecutive tokens of one index of ep, a row holds at most 48, and every draw has rows that hold exactly 48 of them.
All inputs are finite; a program needn't handle non-finite values.
Results may differ from a plain program's by a relative error of at most 0.02.
Values may be sent and summed in bfloat16 or wider, within the bound.
A program may use at most 64 MiB of HBM per device.

v0:
```python
import jax
import jax.numpy as jnp
from jax import lax
from jax.sharding import Mesh
from jax.sharding import PartitionSpec as P

EP = ("ep_0", "ep_1")


def whole_of(x, axes, dim):
    if not axes:
        return x
    nearer = lax.all_gather(x, axes[-1], axis=dim, tiled=True)
    return whole_of(nearer, axes[:-1], dim)


def shards(tokens, norm_gain, chosen, route_weight, gate_weight, up_weight, down_weight):
    tok_rows, row_width = tokens.shape
    experts, capacity = chosen.shape
    ep_count = lax.axis_size(EP)
    tp_count = lax.axis_size("tp")
    owner_index = lax.axis_index(EP)
    lane_index = lax.axis_index("tp")
    slot_most = 3 * tok_rows // 16
    col_width = row_width // tp_count
    values = tokens.astype(jnp.float32)
    scale = lax.rsqrt(jnp.mean(values * values, axis=-1, keepdims=True) + 1e-06)
    normed = (values * scale * norm_gain[None, :]).astype(jnp.bfloat16)
    slot_steps = jnp.arange(slot_most, dtype=jnp.int32)
    first_token = owner_index * tok_rows
    run_start = jnp.sum((chosen < first_token).astype(jnp.int32), axis=1)
    run_end = jnp.sum((chosen < first_token + tok_rows).astype(jnp.int32), axis=1)
    run_count = run_end - run_start
    slot_live = slot_steps[None, :] < run_count[:, None]
    slot_place = jnp.minimum(run_start[:, None] + slot_steps[None, :], capacity - 1)
    slot_token = jnp.take_along_axis(chosen, slot_place, axis=1) - first_token
    my_chosen = lax.dynamic_index_in_dim(chosen, owner_index, 0, keepdims=False)
    block_edges = jnp.arange(ep_count, dtype=jnp.int32) * tok_rows
    src_start = jnp.sum((my_chosen[None, :] < block_edges[:, None]).astype(jnp.int32), axis=1)
    src_end = jnp.concatenate([src_start[1:], jnp.full((1,), capacity, jnp.int32)])
    gate_mat = gate_weight[0]
    up_mat = up_weight[0]
    down_mat = down_weight[0]
    my_columns = lax.dynamic_slice_in_dim(normed, lane_index * col_width, col_width, 1)
    all_columns = whole_of(my_columns, EP, 0)
    picked_rows = all_columns[my_chosen]
    segment = lax.all_gather(picked_rows, "tp", axis=1, tiled=True)
    gate_pre = jnp.dot(segment, gate_mat, preferred_element_type=jnp.float32)
    up_pre = jnp.dot(segment, up_mat, preferred_element_type=jnp.float32)
    hidden = (jax.nn.silu(gate_pre) * up_pre).astype(jnp.bfloat16)
    summed_out = lax.psum_scatter(
        lax.dot_general(
            down_mat, hidden, (((0,), (1,)), ((), ())), preferred_element_type=jnp.float32
        ).astype(jnp.bfloat16),
        "tp",
        scatter_dimension=0,
        tiled=True,
    ).astype(jnp.float32)
    weighted = (summed_out.T * route_weight[0][:, None]).astype(jnp.bfloat16)
    back_place = jnp.minimum(src_start[:, None] + slot_steps[None, :], capacity - 1)
    back_live = slot_steps[None, :] < (src_end - src_start)[:, None]
    outgoing_back = jnp.where(
        back_live[:, :, None], weighted[back_place], jnp.zeros((), jnp.bfloat16)
    )
    returned = lax.all_to_all(outgoing_back, EP, split_axis=0, concat_axis=0, tiled=True)
    target_row = jnp.where(slot_live, slot_token, tok_rows).reshape(-1)
    placement = (jnp.arange(tok_rows, dtype=jnp.int32)[:, None] == target_row[None, :]).astype(
        jnp.bfloat16
    )
    combined = jnp.dot(
        placement, returned.reshape(-1, col_width), preferred_element_type=jnp.float32
    )
    return combined.astype(jnp.bfloat16)


def solution(mesh):
    finer = Mesh(mesh.devices.reshape(8, 4, mesh.shape["tp"]), ("ep_0", "ep_1", "tp"))
    in_specs = (
        P(EP, None),
        P(),
        P(),
        P(EP, None),
        P(EP, None, "tp"),
        P(EP, None, "tp"),
        P(EP, "tp", None),
    )
    out_specs = P(EP, "tp")
    return jax.shard_map(
        shards, mesh=finer, in_specs=in_specs, out_specs=out_specs, check_vma=False
    )
```

profile of v0, /device:TPU:1, one launch (start us, length us, event | category | flops | bytes accessed | tf_op | source)
XLA Modules:
  0.0 246.1 jit_solution(2484285183497416496)
XLA Ops:
  6.5 0.0 copy-start
  6.5 0.0 copy-start.1
  6.5 0.0 all-gather.4.cloned.1.call-start
  6.5 1.5 convert_element_type.40
  8.1 1.5 multiply_reduce_fusion
  9.6 0.8 dynamic-slice
  10.4 0.1 fusion.17
  10.5 11.3 %all_gather.9 = bf16[1024,128]{1,0:T(8,128)(2,1)} all-gather(bf16[256,128]{1,0:T(8,128)(2,1)S(1)} %fusion.17), channel_id=1, replica_groups=mesh['ep_0'=8,'ep_1'=4,'tp'=16] {'ep_1'}, dimensions={0}, use_global_device_ids=true | all-gather | bytes 327680 | tf_op jit(solution)/shard_map/all_gather | solution.py:13
  21.8 0.0 all-gather.4.cloned.1.call-update
  21.8 0.0 all-gather.6.cloned.1.call-start
  21.9 0.0 copy-done.1
  21.9 47.1 %all-gather.4.cloned.1.call-done = bf16[8192,128]{1,0:T(8,128)(2,1)} async-done(((bf16[1024,128]{1,0:T(8,128)(2,1)}), bf16[8192,128]{1,0:T(8,128)(2,1)}) %all-gather.4.cloned.1.call-update) | async-done | bytes 2097168 | tf_op jit(solution)/shard_map/all_gather | solution.py:13
  69.0 5.9 %gather_fusion = bf16[1024,128]{1,0:T(8,128)(2,1)} fusion(bf16[8192,128]{1,0:T(8,128)(2,1)} %all-gather.4.cloned.1.call-done, s32[1024]{0:T(1024)S(1)} %broadcast_clamp_fusion), kind=kCustom, calls=%fused_computation | custom fusion | bytes 528384 | tf_op jit(solution)/shard_map/gather | solution.py:46
  74.9 0.0 copy-start.3
  74.9 0.0 all-gather.6.cloned.1.call-update
  75.0 0.0 reduce-scatter.4.cloned.1.call-start
  75.0 55.4 %all-gather.6.cloned.1.call-done = bf16[1024,2048]{1,0:T(8,128)(2,1)} async-done(((bf16[1024,128]{1,0:T(8,128)(2,1)}), bf16[1024,2048]{1,0:T(8,128)(2,1)}) %all-gather.6.cloned.1.call-update) | async-done | bytes 4194320 | tf_op jit(solution)/shard_map/all_gather | solution.py:47
  130.4 3.7 %fusion.6 = f32[1024,256]{1,0:T(8,128)S(1)} fusion(bf16[1024,2048]{1,0:T(8,128)(2,1)} %all-gather.6.cloned.1.call-done, bf16[1,2048,256]{2,1,0:T(8,128)(2,1)} %param.11), kind=kOutput, calls=%fused_computation.12 | convolution fusion | flops 1073741824 | bytes 6291456 | tf_op jit(solution)/shard_map/dot_general | solution.py:48
  134.2 0.0 copy-done
  134.2 0.0 copy-done.3
  134.2 8.5 %convert_bitcast_fusion = bf16[2048,1024]{0,1:T(8,128)(2,1)} fusion(bf16[1024,2048]{1,0:T(8,128)(2,1)} %all-gather.6.cloned.1.call-done, bf16[1,256,2048]{2,1,0:T(8,128)(2,1)S(1)} %copy-done, bf16[1,2048,256]{2,1,0:T(8,128)(2,1)S(1)} %copy-done.3, f32[1024,256]{1,0:T(8,128)S(1)} %fusion.6), kind=kOutput, calls=%fused_computation.3 | convolution fusion | flops 2151153664 | bytes 11534336 | tf_op jit(solution)/shard_map/dot_general | solution.py:52
  142.7 6.4 %copy.8 = bf16[2048,1024]{1,0:T(8,128)(2,1)} copy(bf16[2048,1024]{0,1:T(8,128)(2,1)} %convert_bitcast_fusion) | data formatting | bytes 8388608
  149.1 0.0 copy-start.2
  149.1 0.0 reduce-scatter.4.cloned.1.call-update
  149.1 0.2 convert_reduce_fusion
  149.3 0.1 slice.3
  149.4 0.1 compare_select_fusion
  149.5 0.1 reshape.234
  149.6 0.1 add_subtract_fusion
  149.6 0.1 iota_compare_fusion.4
  149.7 60.8 %reduce-scatter.4.cloned.1.call-done = bf16[128,1024]{1,0:T(8,128)(2,1)} async-done(((bf16[2048,1024]{1,0:T(8,128)(2,1)}), bf16[128,1024]{1,0:T(8,128)(2,1)}) %reduce-scatter.4.cloned.1.call-update) | async-done | bytes 262160
  210.5 1.1 copy.9
  211.6 0.0 copy-done.2
  211.6 0.2 fusion.15
  211.8 3.2 %gather_fusion.1 = bf16[1536,128]{1,0:T(8,128)(2,1)S(1)} fusion(bf16[1024,128]{1,0:T(8,128)(2,1)S(1)} %fusion.15, s32[2048]{0:T(1024)S(1)} %pad_clamp_fusion), kind=kCustom, calls=%fused_computation.1 | custom fusion | bytes 792576 | tf_op jit(solution)/shard_map/gather | solution.py:63
  215.0 1.0 broadcast_select_fusion
  216.1 9.1 %all-to-all-start = ((bf16[32,48,128]{2,1,0:T(8,128)(2,1)}), bf16[32,48,128]{2,1,0:T(8,128)(2,1)S(1)}, u32[]{:S(2)}, u32[]{:S(2)}) async-start(bf16[32,48,128]{2,1,0:T(8,128)(2,1)} %broadcast_select_fusion), calls=%async_computation | async-start | bytes 786432 | tf_op jit(solution)/shard_map/all_to_all | solution.py:65
  225.2 0.1 convert_reduce_fusion.1
  225.3 0.1 iota_compare_fusion.5
  225.4 0.1 lt.135
  225.5 0.1 fusion.20
  225.6 0.1 reshape.240
  225.7 12.6 %gather_fusion.2 = s32[1536]{0:T(1024)S(1)} fusion(s32[32,1024]{1,0:T(8,128)S(1)} %copy-done.1, s32[1536]{0:T(1024)S(1)} %reshape.240), kind=kCustom, calls=%fused_computation.2 | custom fusion | bytes 24576 | tf_op jit(solution)/shard_map/jit(take_along_axis)/gather | solution.py:36
  238.3 0.1 add.129
  238.4 0.1 add.130
  238.5 0.1 lt.137
  238.5 0.0 all-to-all-done
  238.6 1.0 fusion.2
  (8 shorter events, 0.1 us)
Async XLA Ops:
  6.5 127.6 %copy-start = (bf16[1,256,2048]{2,1,0:T(8,128)(2,1)S(1)}, bf16[1,256,2048]{2,1,0:T(8,128)(2,1)}, u32[]{:S(2)}) copy-start(bf16[1,256,2048]{2,1,0:T(8,128)(2,1)} %param.13) | copy-start | bytes 3145732
  6.5 15.3 %copy-start.1 = (s32[32,1024]{1,0:T(8,128)S(1)}, s32[32,1024]{1,0:T(8,128)}, u32[]{:S(2)}) copy-start(s32[32,1024]{1,0:T(8,128)} %param.9) | copy-start | bytes 393220
  6.5 62.5 %all-gather.4.cloned.1.call-start = ((), (), s32[]{:S(2)}) async-start(), calls=%async_computation.2 | async-start | bytes 2359296 | tf_op jit(solution)/shard_map/all_gather | solution.py:13
  21.8 108.6 %all-gather.6.cloned.1.call-start = ((), (), s32[]{:S(2)}) async-start(), calls=%async_computation.3 | async-start | bytes 4456448 | tf_op jit(solution)/shard_map/all_gather | solution.py:47
  74.9 59.2 %copy-start.3 = (bf16[1,2048,256]{2,1,0:T(8,128)(2,1)S(1)}, bf16[1,2048,256]{2,1,0:T(8,128)(2,1)}, u32[]{:S(2)}) copy-start(bf16[1,2048,256]{2,1,0:T(8,128)(2,1)} %param.12) | copy-start | bytes 3145732
  75.0 135.5 %reduce-scatter.4.cloned.1.call-start = ((), (), s32[]{:S(2)}) async-start(), calls=%async_computation.4 | async-start | bytes 4456448
  149.1 62.5 %copy-start.2 = (f32[1,1024]{1,0:T(1,128)S(1)}, f32[1,1024]{1,0:T(1,128)}, u32[]{:S(2)}) copy-start(f32[1,1024]{1,0:T(1,128)} %param.10) | copy-start | bytes 12292
  216.1 22.5 %all-to-all-start = ((bf16[32,48,128]{2,1,0:T(8,128)(2,1)}), bf16[32,48,128]{2,1,0:T(8,128)(2,1)S(1)}, u32[]{:S(2)}, u32[]{:S(2)}) async-start(bf16[32,48,128]{2,1,0:T(8,128)(2,1)} %broadcast_select_fusion), calls=%async_computation | async-start | bytes 786432 | tf_op jit(solution)/shard_map/all_to_all | solution.py:65
Sparse Core Ops, SparseCore 0:
  21.9 47.0 all-gather.3
  75.1 55.2 all-gather.5
  149.2 61.1 reduce-scatter.3
where the time goes:
time: 249 us; the launch traced here: 246 us
  waiting for transfers between devices  163 us (65%)
  local copies, waits for them, and re-layouts  30.6 us (12%)
  matrix products  13.3 us (5%)
  between operations  13.3 us (5%)
  blocking collectives  11.3 us (5%)
  starting transfers between devices  9.2 us (4%)
  other arithmetic  5.16 us (2%)
    unnamed x4, waiting for transfers between devices  60.8 us
    all_gather x1, waiting for transfers between devices, shards(): segment = lax.all_gather(picked_rows, 'tp', axis=1, tiled=True)  55.4 us
    all_gather x1, waiting for transfers between devices, whole_of(): nearer = lax.all_gather(x, axes[-1], axis=dim, tiled=True)  47.1 us
    gather x2, local copies, waits for them, and re-layouts, shards(): slot_token = jnp.take_along_axis(chosen, slot_place, axis=1) - first_token  12.7 us
    all_gather x1, blocking collectives, whole_of(): nearer = lax.all_gather(x, axes[-1], axis=dim, tiled=True)  11.3 us
    all_to_all x1, starting transfers between devices, shards(): lax.all_to_all(outgoing_back, EP, split_axis=0, concat_axis=0, tiled=True)  9.12 us
    dot_general x1, matrix products, shards(): lax.dot_general(down_mat, hidden, (((0,), (1,)), ((), ())), preferred_ele...  8.52 us
    unnamed x10, local copies, waits for them, and re-layouts  7.53 us
  transfers between devices with their start and end apart: 4, of which 3 were waited for; matrix products, arithmetic and copies ran while one was open for 6% of the time, Pallas kernels for 0%

commit v1 on v0

v1 whole, which is shorter than its diff:
```python
import functools

import jax
import jax.numpy as jnp
from jax import lax
from jax.experimental import pallas as pl
from jax.experimental.pallas import tpu as pltpu
from jax.sharding import Mesh
from jax.sharding import PartitionSpec as P

NZ, NX, NY, NC = 8, 4, 8, 2
EP = NZ * NX
BF = jnp.bfloat16
F32 = jnp.float32
LANES = 128
COPY = pltpu.make_async_copy


def remote(src, dst, send, recv, where):
    return pltpu.make_async_remote_copy(
        src_ref=src, dst_ref=dst, send_sem=send, recv_sem=recv,
        device_id=where, device_id_type=pl.DeviceIdType.MESH,
    )


def hops_of(way, half):
    return NY // 2 if way == half else NY // 2 - 1


def kernel(
    slots, tokens, gain, slot_tok, flat, rw, gate, up, down, out,
    tok_v, gu_v, dw_v, place, unpack, sendbuf, recvbuf, ag, acc, hidden, part, rs_first, rs, back, ret,
    tok_sem, w_sem, wx_send, wx_recv, ep_send, ep_recv, ag_send, ag_recv, rs_send, rs_recv, ret_send, ret_recv,
):
    z, x = lax.axis_index("z"), lax.axis_index("x")
    y, c = lax.axis_index("y"), lax.axis_index("c")
    block = z * NX + x
    rows = ag.shape[2]
    width = 2 * LANES
    ff = gate.shape[1]
    model = tokens.shape[1]
    half_slots = EP * slots

    def wrap(v):
        return lax.rem(v + NY, NY)

    def chip(index, core):
        return (index // NX, lax.rem(index, NX), y, core)

    def along(way):
        return (z, x, wrap(y + 1) if way == 0 else wrap(y - 1), c)

    tok_copy = COPY(tokens, tok_v, tok_sem)
    tok_copy.start()
    own = [
        COPY(gate, gu_v.at[:, pl.ds(0, ff)], w_sem.at[0]),
        COPY(up, gu_v.at[:, pl.ds(ff, ff)], w_sem.at[1]),
        COPY(down, dw_v.at[pl.ds(0, ff), :], w_sem.at[2]),
    ]
    for copy in own:
        copy.start()

    barrier = pltpu.get_barrier_semaphore()
    plane = EP * NC
    me = block * NC + c

    def greet(i, _):
        other = lax.rem(me + i, plane)
        pl.semaphore_signal(
            barrier, inc=1, device_id=chip(other // NC, lax.rem(other, NC)),
            device_id_type=pl.DeviceIdType.MESH,
        )
        return 0

    for way in range(2):
        pl.semaphore_signal(barrier, inc=1, device_id=along(way), device_id_type=pl.DeviceIdType.MESH)
    lax.fori_loop(1, plane, greet, 0)

    token_ids = lax.broadcasted_iota(jnp.int32, (tok_v.shape[0], half_slots), 0)
    for rel in range(2):
        at = pl.ds(rel * half_slots, half_slots)
        place[:, at] = jnp.where(token_ids == slot_tok[:, at], 1.0, 0.0).astype(BF)

    tok_copy.wait()
    squares = jnp.zeros((tok_v.shape[0], 1), F32)
    for part_at in range(0, model, 512):
        values = tok_v[:, pl.ds(part_at, 512)].astype(F32)
        squares = squares + jnp.sum(values * values, axis=-1, keepdims=True)
    scale = lax.rsqrt(squares / model + 1e-06)
    columns = pl.ds(pl.multiple_of(y * width, width), width)
    normed = (tok_v[:, columns].astype(F32) * scale * gain[:, columns]).astype(BF)
    packed = lax.dot_general(
        place[:, pl.ds(0, half_slots)], normed, (((0,), (0,)), ((), ())), preferred_element_type=F32
    )
    for h in range(2):
        sendbuf[h] = packed[:, h * LANES:(h + 1) * LANES].astype(BF).reshape(EP, slots, LANES)

    pl.semaphore_wait(barrier, plane - 1 + 2)

    for h in range(2):
        COPY(sendbuf.at[h, block], recvbuf.at[h, block], ep_recv.at[h]).start()

        def exchange(i, _):
            other = lax.rem(block + i, EP)
            remote(
                sendbuf.at[h, other], recvbuf.at[h, block], ep_send.at[h], ep_recv.at[h], chip(other, c)
            ).start()
            return 0

        lax.fori_loop(1, EP, exchange, 0)

    sibling = (z, x, y, 1 - c)
    shared = [
        remote(gate, gu_v.at[:, pl.ds(2 * ff, ff)], wx_send.at[0], wx_recv.at[0], sibling),
        remote(up, gu_v.at[:, pl.ds(3 * ff, ff)], wx_send.at[1], wx_recv.at[1], sibling),
        remote(down, dw_v.at[pl.ds(ff, ff), :], wx_send.at[2], wx_recv.at[2], sibling),
    ]
    for copy in shared:
        copy.start()

    slot_ids = lax.broadcasted_iota(jnp.int32, (half_slots, rows), 0)
    unpack[...] = jnp.where(slot_ids == flat[...], 1.0, 0.0).astype(BF)

    def ag_copy(way, h, hop):
        source = wrap(y - hop + 1) if way == 0 else wrap(y + hop - 1)
        where = ag.at[h, source]
        return remote(where, where, ag_send.at[way, h, hop - 1], ag_recv.at[way, h, hop - 1], along(way))

    for h in range(2):
        COPY(recvbuf.at[h], recvbuf.at[h], ep_recv.at[h]).wait()
        ag[h, y] = lax.dot_general(
            unpack[...], recvbuf[h].reshape(half_slots, LANES), (((0,), (0,)), ((), ())),
            preferred_element_type=F32,
        ).astype(BF)
        for way in range(2):
            ag_copy(way, h, 1).start()

    for copy in own:
        copy.wait()
    for copy in shared[:2]:
        copy.wait_recv()

    def gather_in(source, first):
        x_rows = jnp.concatenate([ag[0, source], ag[1, source]], axis=1)
        k_at = pl.ds(pl.multiple_of(source * width, width), width)

        def tile(n, _):
            n_at = pl.ds(pl.multiple_of(n * ff, ff), ff)
            product = jnp.dot(x_rows, gu_v[k_at, n_at], preferred_element_type=F32)
            if first:
                acc[:, n_at] = product
            else:
                acc[:, n_at] += product
            return 0

        lax.fori_loop(0, 4, tile, 0)

    gather_in(y, True)
    for hop in range(1, NY // 2 + 1):
        for h in range(2):
            for way in range(2):
                if hop <= hops_of(way, h):
                    ag_copy(way, h, hop).wait_recv()
                    if hop < hops_of(way, h):
                        ag_copy(way, h, hop + 1).start()
        gather_in(wrap(y - hop), False)
        if hop < NY // 2:
            gather_in(wrap(y + hop), False)

    for s in range(2):
        gate_pre = acc[:, pl.ds(2 * s * ff, ff)]
        up_pre = acc[:, pl.ds((2 * s + 1) * ff, ff)]
        hidden[:, pl.ds(s * ff, ff)] = (gate_pre / (1.0 + jnp.exp(-gate_pre)) * up_pre).astype(BF)
    shared[2].wait_recv()

    def partial_of(offset):
        target = wrap(y + offset)
        return jnp.dot(
            hidden[...], dw_v[:, pl.ds(pl.multiple_of(target * width, width), width)],
            preferred_element_type=F32,
        )

    def rs_copy(way, h, hop):
        source = rs_first.at[way, h] if hop == 1 else rs.at[way, h, hop - 2]
        return remote(
            source, rs.at[way, h, hop - 1], rs_send.at[way, h, hop - 1], rs_recv.at[way, h, hop - 1], along(way)
        )

    far = NY // 2
    product = partial_of(far)
    for way in range(2):
        h = way
        rs_first[way, h] = product[:, h * LANES:(h + 1) * LANES].astype(BF)
        rs_copy(way, h, 1).start()
    for way in range(2):
        h = 1 - way
        offset = far - 1 if way == 0 else 1 - far
        product = partial_of(offset)
        rs_first[way, h] = product[:, h * LANES:(h + 1) * LANES].astype(BF)
        rs_copy(way, h, 1).start()
        part[offset % NY] = product
    for offset in (2, -2, 1, -1, 0):
        part[offset % NY] = partial_of(offset)

    for hop in range(1, far):
        for order in range(2):
            for way in range(2):
                h = way if order == 0 else 1 - way
                hops = hops_of(way, h)
                if hop < hops:
                    rs_copy(way, h, hop).wait_recv()
                    offset = hops - hop if way == 0 else hop - hops
                    mine = part[offset % NY, :, pl.ds(h * LANES, LANES)]
                    rs[way, h, hop - 1] = (rs[way, h, hop - 1].astype(F32) + mine).astype(BF)
                    rs_copy(way, h, hop + 1).start()

    factor = jnp.broadcast_to(rw[...], (LANES, rows)).T
    for h in range(2):
        for way in range(2):
            rs_copy(way, h, hops_of(way, h)).wait_recv()
        total = part[0, :, pl.ds(h * LANES, LANES)]
        for way in range(2):
            total = total + rs[way, h, hops_of(way, h) - 1].astype(F32)
        weighted = (total * factor).astype(BF)
        back[h] = (
            jnp.dot(unpack[...], weighted, preferred_element_type=F32).astype(BF).reshape(EP, slots, LANES)
        )
        rel = lax.rem(c + h, 2)

        def give(i, _):
            other = lax.rem(block + i, EP)
            remote(back.at[h, other], ret.at[rel, block], ret_send, ret_recv, chip(other, h)).start()
            return 0

        lax.fori_loop(1, EP, give, 0)

        @pl.when(c == h)
        def _():
            COPY(back.at[h, block], ret.at[rel, block], ret_recv).start()

        @pl.when(c != h)
        def _():
            remote(back.at[h, block], ret.at[rel, block], ret_send, ret_recv, chip(block, h)).start()

    COPY(ret, ret, ret_recv).wait()
    out[...] = jnp.dot(
        place[...], ret[...].reshape(2 * half_slots, LANES), preferred_element_type=F32
    ).astype(BF)

    for h in range(2):
        sent = sendbuf.at[h, pl.ds(0, EP - 1)]
        COPY(sent, sent, ep_send.at[h]).wait()
        for way in range(2):
            for hop in range(1, hops_of(way, h) + 1):
                ag_copy(way, h, hop).wait_send()
                rs_copy(way, h, hop).wait_send()
    for copy in shared:
        copy.wait_send()
    for h in range(2):
        sent = back.at[h, pl.ds(0, EP - h)]
        COPY(sent, sent, ret_send).wait()


def shards(tokens, norm_gain, chosen, route_weight, gate_weight, up_weight, down_weight):
    tok_rows, model = tokens.shape
    experts, capacity = chosen.shape
    ff = gate_weight.shape[2]
    slots = 3 * tok_rows // 32
    rows = capacity // 2
    block = lax.axis_index(("z", "x"))
    c = lax.axis_index("c")

    first = block * tok_rows
    start = jnp.sum((chosen < first).astype(jnp.int32), axis=1)
    end = jnp.sum((chosen < first + tok_rows).astype(jnp.int32), axis=1)
    parity = (c + jnp.arange(2, dtype=jnp.int32)) & 1
    lead = start[None, :] + ((start[None, :] + parity[:, None]) & 1)
    position = lead[:, :, None] + 2 * jnp.arange(slots, dtype=jnp.int32)[None, None, :]
    hit = position[:, :, :, None] == jnp.arange(capacity, dtype=jnp.int32)
    token = jnp.sum(jnp.where(hit, chosen[None, :, None, :] - first, 0), axis=-1)
    slot_tok = jnp.where(position < end[None, :, None], token, -1).reshape(1, -1)

    def mine(row):
        return lax.dynamic_index_in_dim(row.reshape(rows, 2), c, 1, keepdims=False)

    source = mine(lax.dynamic_index_in_dim(chosen, block, 0, keepdims=False)) // tok_rows
    before = jnp.sum((source[:, None] < source[None, :]).astype(jnp.int32), axis=0)
    flat = (source * slots + jnp.arange(rows, dtype=jnp.int32) - before).reshape(1, rows)
    rw = mine(route_weight[0]).reshape(1, rows)

    vmem = pl.BlockSpec(memory_space=pltpu.VMEM)
    hbm = pl.BlockSpec(memory_space=pl.ANY)
    far = NY // 2
    dma = pltpu.SemaphoreType.DMA
    return pl.pallas_call(
        functools.partial(kernel, slots),
        out_shape=jax.ShapeDtypeStruct((tok_rows, model // (NY * NC)), BF),
        in_specs=[hbm, vmem, vmem, vmem, vmem, hbm, hbm, hbm],
        out_specs=vmem,
        scratch_shapes=[
            pltpu.VMEM((tok_rows, model), BF),
            pltpu.VMEM((model, 4 * ff), BF),
            pltpu.VMEM((2 * ff, model), BF),
            pltpu.VMEM((tok_rows, 2 * EP * slots), BF),
            pltpu.VMEM((EP * slots, rows), BF),
            pltpu.VMEM((2, EP, slots, LANES), BF),
            pltpu.VMEM((2, EP, slots, LANES), BF),
            pltpu.VMEM((2, NY, rows, LANES), BF),
            pltpu.VMEM((rows, 4 * ff), F32),
            pltpu.VMEM((rows, 2 * ff), BF),
            pltpu.VMEM((NY, rows, 2 * LANES), F32),
            pltpu.VMEM((2, 2, rows, LANES), BF),
            pltpu.VMEM((2, 2, far, rows, LANES), BF),
            pltpu.VMEM((2, EP, slots, LANES), BF),
            pltpu.VMEM((2, EP, slots, LANES), BF),
            dma(()),
            dma((3,)),
            dma((3,)),
            dma((3,)),
            dma((2,)),
            dma((2,)),
            dma((2, 2, far)),
            dma((2, 2, far)),
            dma((2, 2, far)),
            dma((2, 2, far)),
            dma(()),
            dma(()),
        ],
        compiler_params=pltpu.CompilerParams(
            collective_id=0, has_side_effects=True, vmem_limit_bytes=56 * 1024 * 1024
        ),
    )(tokens, norm_gain.reshape(1, -1), slot_tok, flat, rw, gate_weight[0], up_weight[0], down_weight[0])


def solution(mesh):
    finer = Mesh(mesh.devices.reshape(NZ, NX, NY, NC), ("z", "x", "y", "c"))
    ep, tp = ("z", "x"), ("y", "c")
    in_specs = (
        P(ep, None),
        P(),
        P(),
        P(ep, None),
        P(ep, None, tp),
        P(ep, None, tp),
        P(ep, tp, None),
    )
    return jax.shard_map(
        shards, mesh=finer, in_specs=in_specs, out_specs=P(ep, tp), check_vma=False
    )
```

time: 249 us -> 94.4 us (0.38); the launches traced: 246 us -> 94.1 us
  waiting for transfers between devices: 163 us -> 0 us
  Pallas kernels: 0 us -> 84.6 us
  local copies, waits for them, and re-layouts: 30.6 us -> 4.76 us
  matrix products: 13.3 us -> 0 us
  between operations: 13.3 us -> 0.06 us
  blocking collectives: 11.3 us -> 0 us
  starting transfers between devices: 9.2 us -> 0 us
    all_gather x2 -> x0, waiting for transfers between devices: 103 us -> none  [the longest x1 55.4 us: shards(): segment = lax.all_gather(picked_rows, 'tp', axis=1, tiled=True)]
    pallas_call x0 -> x1, Pallas kernels: none -> 84.6 us  [shards(): pl.pallas_call(functools.partial(kernel, slots), out_shape=jax.ShapeDtype...]
    unnamed x4 -> x0, waiting for transfers between devices: 60.8 us -> none
    gather x4 -> x0, local copies, waits for them, and re-layouts: 21.8 us -> none  [the longest x2 12.7 us: shards(): slot_token = jnp.take_along_axis(chosen, slot_place, axis=1) - first_token]
    dot_general x3 -> x0, matrix products: 13.3 us -> none  [the longest x1 8.52 us: shards(): lax.dot_general(down_mat, hidden, (((0,), (1,)), ((), ())), preferred_ele...]
    all_gather x1 -> x0, blocking collectives: 11.3 us -> none  [whole_of(): nearer = lax.all_gather(x, axes[-1], axis=dim, tiled=True)]
    all_to_all x1 -> x0, starting transfers between devices: 9.12 us -> none  [shards(): lax.all_to_all(outgoing_back, EP, split_axis=0, concat_axis=0, tiled=True)]
    unnamed x10 -> x4, local copies, waits for them, and re-layouts: 7.53 us -> 2.07 us
  transfers between devices with their start and end apart: 4 -> 0, of which waited for: 3 -> 0; matrix products, arithmetic and copies ran while one was open for 6% -> 0% of each run, Pallas kernels for 0% -> 0%
where the time goes in v1:
time: 94.4 us; the launch traced here: 94.1 us
  Pallas kernels  84.6 us (90%)
  local copies, waits for them, and re-layouts  4.76 us (5%)
  other arithmetic  4.72 us (5%)
    pallas_call x1, Pallas kernels, shards(): pl.pallas_call(functools.partial(kernel, slots), out_shape=jax.ShapeDtype...  84.6 us
    unnamed x4, local copies, waits for them, and re-layouts  2.07 us

profile of v1, /device:TPU:1, one launch (start us, length us, event | category | flops | bytes accessed | tf_op | source)
XLA Modules:
  0.0 94.1 jit_solution(11350565311639721071)
XLA Ops:
  0.0 0.0 copy-start
  0.0 0.8 dynamic-slice_reduce_fusion.2
  0.8 0.2 reshape.208
  1.0 0.4 fusion.1
  1.4 0.2 convert_reduce_fusion
  1.6 0.6 add_subtract_fusion.flat
  2.2 1.0 %convert_reduce_fusion.1 = (s32[32]{0:T(128)S(1)}, s32[32]{0:T(128)S(1)}, s32[32,1024]{1,0:T(8,128)S(1)}) fusion(s32[32,1024]{1,0:T(8,128)} %param.9, s32[]{:T(128)S(6)} %add.110, s32[]{:T(128)S(6)} %mul.28), kind=kLoop, calls=%fused_computation.13 | loop fusion | flops 229312 | bytes 262408 | tf_op jit(solution)/shard_map/reduce_sum | solution.py:275
  3.2 0.1 and_add_fusion
  3.3 0.1 broadcast_add_fusion
  3.4 1.6 %select_reduce_fusion = s32[2,32,24]{2,1,0:T(8,128)S(1)} fusion(s32[32,1024]{1,0:T(8,128)S(1)} %get-tuple-element.9, s32[2,32,24]{2,1,0:T(8,128)S(1)} %broadcast_add_fusion), kind=kLoop, calls=%fused_computation | loop fusion | flops 4717056 | bytes 143360 | tf_op jit(solution)/shard_map/reduce_sum | solution.py:280
  5.0 0.1 compare_select_fusion
  5.0 0.7 select_n.50.slot_tok
  5.7 0.6 broadcast.193
  6.3 0.0 copy-done
  6.3 0.7 reduce.14
  7.0 0.2 reshape_squeeze.3
  7.2 0.8 dynamic-slice_reduce_fusion
  8.1 84.6 %shard_map.73 = bf16[256,128]{1,0:T(8,128)(2,1)} custom-call(bf16[256,2048]{1,0:T(8,128)(2,1)} %tokens.1, f32[1,2048]{1,0:T(1,128)} %bitcast.11, s32[1,1536]{1,0:T(1,128)} %select_n.50.slot_tok, s32[1,512]{1,0:T(1,128)} %add_subtract_fusion.flat, f32[1,512]{1,0:T(1,128)} %bitcast.12, bf16[2048,256]{1,0:T(8,128)(2,1)} %bitcast.7, bf16[2048,256]{1,0:T(8,128)(2,1)} %bitcast.8, ...), custom_call_target="tpu_custom_call" | custom-call | tf_op jit(solution)/shard_map/pallas_call | solution.py:295
  92.6 1.5 %copy.9 = bf16[256,128]{1,0:T(8,128)(2,1)} copy(bf16[256,128]{1,0:T(8,128)(2,1)} %shard_map.73) | data formatting | bytes 131072
  (3 shorter events, 0.0 us)
Async XLA Ops:
  0.0 6.3 %copy-start = (f32[1,1024]{1,0:T(1,128)S(1)}, f32[1,1024]{1,0:T(1,128)}, u32[]{:S(2)}) copy-start(f32[1,1024]{1,0:T(1,128)} %param.10) | copy-start | bytes 12292

commit v2 on v1

--- a/solution.py
+++ b/solution.py
@@ -28,8 +28,8 @@
 
 
 def kernel(
-    slots, tokens, gain, slot_tok, flat, rw, gate, up, down, out,
-    tok_v, gu_v, dw_v, place, unpack, sendbuf, recvbuf, ag, acc, hidden, part, rs_first, rs, back, ret,
+    slots, tokens, gain, chosen, rw, gate, up, down, out,
+    tok_v, gu_v, dw_v, values, dist, rank, factor, place, place_t, unpack, unpack_t, sendbuf, recvbuf, ag, acc, hidden, part, rs_first, rs, back, ret,
     tok_sem, w_sem, wx_send, wx_recv, ep_send, ep_recv, ag_send, ag_recv, rs_send, rs_recv, ret_send, ret_recv,
 ):
     z, x = lax.axis_index("z"), lax.axis_index("x")
@@ -76,22 +76,79 @@
         pl.semaphore_signal(barrier, inc=1, device_id=along(way), device_id_type=pl.DeviceIdType.MESH)
     lax.fori_loop(1, plane, greet, 0)
 
-    token_ids = lax.broadcasted_iota(jnp.int32, (tok_v.shape[0], half_slots), 0)
-    for rel in range(2):
-        at = pl.ds(rel * half_slots, half_slots)
-        place[:, at] = jnp.where(token_ids == slot_tok[:, at], 1.0, 0.0).astype(BF)
-
+    tok_rows, capacity = tok_v.shape[0], chosen.shape[1]
+    first = block * tok_rows
+    pair = 2 * slots
+    slot_steps = lax.broadcasted_iota(jnp.int32, (slots, 1), 0)
+    positions = lax.broadcasted_iota(jnp.int32, (1, capacity), 1)
+
+    def count(hits):
+        return jnp.sum(jnp.where(hits, 1.0, 0.0), axis=1, keepdims=True).astype(jnp.int32)
+
+    run_start = count(chosen[...] < first)
+    values[...] = (chosen[...] - (first - 1)).astype(F32)
+    token_ids = (lax.broadcasted_iota(jnp.int32, (1, tok_rows), 1) + 1).astype(F32)
+
+    def build_place(rel):
+        parity = lax.rem(c + rel, 2)
+        lead = run_start + ((run_start + parity) & 1)
+        dist[...] = positions - lead
+
+        def body(i, _):
+            made = []
+            for k in range(2):
+                at = pl.ds(2 * i + k, 1)
+                found = jnp.where(dist[at, :] == 2 * slot_steps, values[at, :], 0.0)
+                token = jnp.sum(found, axis=1, keepdims=True)
+                made.append(jnp.where(token == token_ids, 1.0, 0.0))
+            to = pl.ds(pl.multiple_of(rel * half_slots + i * pair, pair), pair)
+            place[to, :] = jnp.concatenate(made, axis=0).astype(BF)
+            return 0
+
+        lax.fori_loop(0, EP // 2, body, 0, unroll=4)
+
+    def build_unpack():
+        edges = lax.broadcasted_iota(jnp.int32, (EP, 1), 0) * tok_rows
+        row = chosen[pl.ds(block, 1), :]
+        lo, hi = count(row < edges), count(row < edges + tok_rows)
+        lead = lo + ((lo + c) & 1)
+        base = (lead - c) >> 1
+        filled = (hi - lead + 1) >> 1
+        ahead = lax.broadcasted_iota(jnp.int32, (1, rows), 1) - base
+        rank[...] = jnp.where((ahead >= 0) & (ahead < filled), ahead, -1)
+
+        def body(i, _):
+            made = [
+                jnp.where(rank[pl.ds(2 * i + k, 1), :] == slot_steps, 1.0, 0.0) for k in range(2)
+            ]
+            unpack[pl.ds(pl.multiple_of(i * pair, pair), pair), :] = jnp.concatenate(made, axis=0).astype(BF)
+            return 0
+
+        lax.fori_loop(0, EP // 2, body, 0, unroll=4)
+        unpack_t[...] = unpack[...].T
+
+    def build_factor():
+        step = min(LANES, rows)
+
+        def body(i, _):
+            at = pl.ds(pl.multiple_of(i * step, step), step)
+            wanted = 2 * (lax.broadcasted_iota(jnp.int32, (step, 1), 0) + i * step) + c
+            found = jnp.where(positions == wanted, rw[...], 0.0)
+            factor[at, :] = jnp.broadcast_to(jnp.sum(found, axis=1, keepdims=True), (step, LANES))
+            return 0
+
+        lax.fori_loop(0, rows // step, body, 0)
+
+    build_place(0)
     tok_copy.wait()
     squares = jnp.zeros((tok_v.shape[0], 1), F32)
     for part_at in range(0, model, 512):
-        values = tok_v[:, pl.ds(part_at, 512)].astype(F32)
-        squares = squares + jnp.sum(values * values, axis=-1, keepdims=True)
+        some = tok_v[:, pl.ds(part_at, 512)].astype(F32)
+        squares = squares + jnp.sum(some * some, axis=-1, keepdims=True)
     scale = lax.rsqrt(squares / model + 1e-06)
     columns = pl.ds(pl.multiple_of(y * width, width), width)
     normed = (tok_v[:, columns].astype(F32) * scale * gain[:, columns]).astype(BF)
-    packed = lax.dot_general(
-        place[:, pl.ds(0, half_slots)], normed, (((0,), (0,)), ((), ())), preferred_element_type=F32
-    )
+    packed = jnp.dot(place[pl.ds(0, half_slots), :], normed, preferred_element_type=F32)
     for h in range(2):
         sendbuf[h] = packed[:, h * LANES:(h + 1) * LANES].astype(BF).reshape(EP, slots, LANES)
 
@@ -118,8 +175,7 @@
     for copy in shared:
         copy.start()
 
-    slot_ids = lax.broadcasted_iota(jnp.int32, (half_slots, rows), 0)
-    unpack[...] = jnp.where(slot_ids == flat[...], 1.0, 0.0).astype(BF)
+    build_unpack()
 
     def ag_copy(way, h, hop):
         source = wrap(y - hop + 1) if way == 0 else wrap(y + hop - 1)
@@ -128,9 +184,8 @@
 
     for h in range(2):
         COPY(recvbuf.at[h], recvbuf.at[h], ep_recv.at[h]).wait()
-        ag[h, y] = lax.dot_general(
-            unpack[...], recvbuf[h].reshape(half_slots, LANES), (((0,), (0,)), ((), ())),
-            preferred_element_type=F32,
+        ag[h, y] = jnp.dot(
+            unpack_t[...], recvbuf[h].reshape(half_slots, LANES), preferred_element_type=F32
         ).astype(BF)
         for way in range(2):
             ag_copy(way, h, 1).start()
@@ -156,6 +211,9 @@
         lax.fori_loop(0, 4, tile, 0)
 
     gather_in(y, True)
+    build_factor()
+    build_place(1)
+    place_t[...] = place[...].T
     for hop in range(1, NY // 2 + 1):
         for h in range(2):
             for way in range(2):
@@ -214,14 +272,13 @@
                     rs[way, h, hop - 1] = (rs[way, h, hop - 1].astype(F32) + mine).astype(BF)
                     rs_copy(way, h, hop + 1).start()
 
-    factor = jnp.broadcast_to(rw[...], (LANES, rows)).T
     for h in range(2):
         for way in range(2):
             rs_copy(way, h, hops_of(way, h)).wait_recv()
         total = part[0, :, pl.ds(h * LANES, LANES)]
         for way in range(2):
             total = total + rs[way, h, hops_of(way, h) - 1].astype(F32)
-        weighted = (total * factor).astype(BF)
+        weighted = (total * factor[...]).astype(BF)
         back[h] = (
             jnp.dot(unpack[...], weighted, preferred_element_type=F32).astype(BF).reshape(EP, slots, LANES)
         )
@@ -244,7 +301,7 @@
 
     COPY(ret, ret, ret_recv).wait()
     out[...] = jnp.dot(
-        place[...], ret[...].reshape(2 * half_slots, LANES), preferred_element_type=F32
+        place_t[...], ret[...].reshape(2 * half_slots, LANES), preferred_element_type=F32
     ).astype(BF)
 
     for h in range(2):
@@ -267,27 +324,6 @@
     ff = gate_weight.shape[2]
     slots = 3 * tok_rows // 32
     rows = capacity // 2
-    block = lax.axis_index(("z", "x"))
-    c = lax.axis_index("c")
-
-    first = block * tok_rows
-    start = jnp.sum((chosen < first).astype(jnp.int32), axis=1)
-    end = jnp.sum((chosen < first + tok_rows).astype(jnp.int32), axis=1)
-    parity = (c + jnp.arange(2, dtype=jnp.int32)) & 1
-    lead = start[None, :] + ((start[None, :] + parity[:, None]) & 1)
-    position = lead[:, :, None] + 2 * jnp.arange(slots, dtype=jnp.int32)[None, None, :]
-    hit = position[:, :, :, None] == jnp.arange(capacity, dtype=jnp.int32)
-    token = jnp.sum(jnp.where(hit, chosen[None, :, None, :] - first, 0), axis=-1)
-    slot_tok = jnp.where(position < end[None, :, None], token, -1).reshape(1, -1)
-
-    def mine(row):
-        return lax.dynamic_index_in_dim(row.reshape(rows, 2), c, 1, keepdims=False)
-
-    source = mine(lax.dynamic_index_in_dim(chosen, block, 0, keepdims=False)) // tok_rows
-    before = jnp.sum((source[:, None] < source[None, :]).astype(jnp.int32), axis=0)
-    flat = (source * slots + jnp.arange(rows, dtype=jnp.int32) - before).reshape(1, rows)
-    rw = mine(route_weight[0]).reshape(1, rows)
-
     vmem = pl.BlockSpec(memory_space=pltpu.VMEM)
     hbm = pl.BlockSpec(memory_space=pl.ANY)
     far = NY // 2
@@ -295,14 +331,20 @@
     return pl.pallas_call(
         functools.partial(kernel, slots),
         out_shape=jax.ShapeDtypeStruct((tok_rows, model // (NY * NC)), BF),
-        in_specs=[hbm, vmem, vmem, vmem, vmem, hbm, hbm, hbm],
+        in_specs=[hbm, vmem, vmem, vmem, hbm, hbm, hbm],
         out_specs=vmem,
         scratch_shapes=[
             pltpu.VMEM((tok_rows, model), BF),
             pltpu.VMEM((model, 4 * ff), BF),
             pltpu.VMEM((2 * ff, model), BF),
+            pltpu.VMEM((experts, capacity), F32),
+            pltpu.VMEM((experts, capacity), jnp.int32),
+            pltpu.VMEM((EP, rows), jnp.int32),
+            pltpu.VMEM((rows, LANES), F32),
+            pltpu.VMEM((2 * EP * slots, tok_rows), BF),
             pltpu.VMEM((tok_rows, 2 * EP * slots), BF),
             pltpu.VMEM((EP * slots, rows), BF),
+            pltpu.VMEM((rows, EP * slots), BF),
             pltpu.VMEM((2, EP, slots, LANES), BF),
             pltpu.VMEM((2, EP, slots, LANES), BF),
             pltpu.VMEM((2, NY, rows, LANES), BF),
@@ -329,7 +371,7 @@
         compiler_params=pltpu.CompilerParams(
             collective_id=0, has_side_effects=True, vmem_limit_bytes=56 * 1024 * 1024
         ),
-    )(tokens, norm_gain.reshape(1, -1), slot_tok, flat, rw, gate_weight[0], up_weight[0], down_weight[0])
+    )(tokens, norm_gain.reshape(1, -1), chosen, route_weight, gate_weight[0], up_weight[0], down_weight[0])
 
 
 def solution(mesh):

time: 94.4 us -> 86.6 us (0.917)
  other arithmetic: 4.72 us -> 0 us
  local copies, waits for them, and re-layouts: 4.76 us -> 1.47 us
    reduce_sum x3 -> x0, other arithmetic: 2.79 us -> none  [the longest x1 1.57 us: shards(): jnp.sum(jnp.where(hit, chosen[None, :, None, :] - first, 0), axis=-1)]
    dynamic_slice x2 -> x0, local copies, waits for them, and re-layouts: 1.6 us -> none  [the longest x1 0.82 us: mine(): return lax.dynamic_index_in_dim(row.reshape(rows, 2), c, 1, keepdims=False)]
    unnamed x4 -> x1, local copies, waits for them, and re-layouts: 2.07 us -> 1.47 us
where the time goes in v2:
time: 86.6 us; the launch traced here: 86.4 us
  Pallas kernels  84.9 us (98%)
  local copies, waits for them, and re-layouts  1.47 us (2%)
    pallas_call x1, Pallas kernels, shards(): pl.pallas_call(functools.partial(kernel, slots), out_shape=jax.ShapeDtype...  84.9 us

profile of v2, /device:TPU:1, one launch (start us, length us, event | category | flops | bytes accessed | tf_op | source)
XLA Modules:
  0.0 86.4 jit_solution(13712593648184494276)
XLA Ops:
  0.0 84.9 %shard_map.73 = bf16[256,128]{1,0:T(8,128)(2,1)} custom-call(bf16[256,2048]{1,0:T(8,128)(2,1)} %tokens.1, f32[1,2048]{1,0:T(1,128)} %bitcast.7, s32[32,1024]{1,0:T(8,128)} %chosen.1, f32[1,1024]{1,0:T(1,128)} %rw.1, bf16[2048,256]{1,0:T(8,128)(2,1)} %bitcast.4, bf16[2048,256]{1,0:T(8,128)(2,1)} %bitcast.5, bf16[256,2048]{1,0:T(8,128)(2,1)} %bitcast.6), custom_call_target="tpu_custom_call" | custom-call | tf_op jit(solution)/shard_map/pallas_call | solution.py:331
  84.9 1.5 %copy.9 = bf16[256,128]{1,0:T(8,128)(2,1)} copy(bf16[256,128]{1,0:T(8,128)(2,1)} %shard_map.73) | data formatting | bytes 131072

commit v3 on v2

v3 whole, which is shorter than its diff:
```python
import functools

import jax
import jax.numpy as jnp
from jax import lax
from jax.experimental import pallas as pl
from jax.experimental.pallas import tpu as pltpu
from jax.sharding import Mesh
from jax.sharding import PartitionSpec as P

NZ, NX, NY, NC = 8, 4, 8, 2
EP = NZ * NX
BF = jnp.bfloat16
F32 = jnp.float32
LANES = 128
COPY = pltpu.make_async_copy


def remote(src, dst, send, recv, where):
    return pltpu.make_async_remote_copy(
        src_ref=src, dst_ref=dst, send_sem=send, recv_sem=recv,
        device_id=where, device_id_type=pl.DeviceIdType.MESH,
    )


FAR = NY // 2


def kernel(
    slots, tokens, gain_in, chosen_in, rw_in, gate, up, down, out,
    tok_v, gain, chosen, rw, gu_v, dw_v, values, dist, rank, factor, place, place_t, unpack, unpack_t, sendbuf, recvbuf, ag, acc, hidden, part, rs_first, rs, back, ret,
    tok_sem, in_sem, w_sem, wx_send, wx_recv, ep_send, ep_recv, ag_send, ag_recv, rs_send, rs_recv, ret_send, ret_recv,
):
    z, x = lax.axis_index("z"), lax.axis_index("x")
    y, c = lax.axis_index("y"), lax.axis_index("c")
    block = z * NX + x
    rows = ag.shape[2]
    width = 2 * LANES
    ff = gate.shape[1]
    model = tokens.shape[1]
    half_slots = EP * slots

    def wrap(v):
        return lax.rem(v + NY, NY)

    def chip(index, core):
        return (index // NX, lax.rem(index, NX), y, core)

    def along(way):
        return (z, x, wrap(y + 1) if way == 0 else wrap(y - 1), c)

    small = [
        COPY(chosen_in, chosen, in_sem.at[0]),
        COPY(gain_in, gain, in_sem.at[1]),
        COPY(rw_in, rw, in_sem.at[2]),
    ]
    small[0].start()
    tok_copy = COPY(tokens, tok_v, tok_sem)
    tok_copy.start()
    for copy in small[1:]:
        copy.start()
    own = [
        COPY(gate, gu_v.at[:, pl.ds(0, ff)], w_sem.at[0]),
        COPY(up, gu_v.at[:, pl.ds(ff, ff)], w_sem.at[1]),
        COPY(down, dw_v.at[pl.ds(0, ff), :], w_sem.at[2]),
    ]
    for copy in own:
        copy.start()

    def peer(i):
        k, r = (i - 1) // NX, lax.rem(i - 1, NX)
        away = NZ // 2 - (k + 1) // 2
        dz = jnp.where(lax.rem(k, 2) == 0, NZ - away, away)
        return lax.rem(z + dz, NZ) * NX + lax.rem(x + NX - 1 - r, NX)

    barrier = pltpu.get_barrier_semaphore()
    plane = EP * NC
    me = block * NC + c

    def greet(i, _):
        other = lax.rem(me + i, plane)
        pl.semaphore_signal(
            barrier, inc=1, device_id=chip(other // NC, lax.rem(other, NC)),
            device_id_type=pl.DeviceIdType.MESH,
        )
        return 0

    for way in range(2):
        pl.semaphore_signal(barrier, inc=1, device_id=along(way), device_id_type=pl.DeviceIdType.MESH)
    lax.fori_loop(1, plane, greet, 0)

    tok_rows, capacity = tok_v.shape[0], chosen.shape[1]
    first = block * tok_rows
    pair = 2 * slots
    slot_steps = lax.broadcasted_iota(jnp.int32, (slots, 1), 0)
    positions = lax.broadcasted_iota(jnp.int32, (1, capacity), 1)

    def count(hits):
        return jnp.sum(jnp.where(hits, 1.0, 0.0), axis=1, keepdims=True).astype(jnp.int32)

    small[0].wait()
    run_start = count(chosen[...] < first)
    values[...] = (chosen[...] - (first - 1)).astype(F32)
    token_ids = (lax.broadcasted_iota(jnp.int32, (1, tok_rows), 1) + 1).astype(F32)

    def build_place(rel):
        parity = lax.rem(c + rel, 2)
        lead = run_start + ((run_start + parity) & 1)
        dist[...] = positions - lead

        def body(i, _):
            made = []
            for k in range(2):
                at = pl.ds(2 * i + k, 1)
                found = jnp.where(dist[at, :] == 2 * slot_steps, values[at, :], 0.0)
                token = jnp.sum(found, axis=1, keepdims=True)
                made.append(jnp.where(token == token_ids, 1.0, 0.0))
            to = pl.ds(pl.multiple_of(rel * half_slots + i * pair, pair), pair)
            place[to, :] = jnp.concatenate(made, axis=0).astype(BF)
            return 0

        lax.fori_loop(0, EP // 2, body, 0, unroll=4)

    def build_unpack():
        edges = lax.broadcasted_iota(jnp.int32, (EP, 1), 0) * tok_rows
        row = chosen[pl.ds(block, 1), :]
        lo, hi = count(row < edges), count(row < edges + tok_rows)
        lead = lo + ((lo + c) & 1)
        base = (lead - c) >> 1
        filled = (hi - lead + 1) >> 1
        ahead = lax.broadcasted_iota(jnp.int32, (1, rows), 1) - base
        rank[...] = jnp.where((ahead >= 0) & (ahead < filled), ahead, -1)

        def body(i, _):
            made = [
                jnp.where(rank[pl.ds(2 * i + k, 1), :] == slot_steps, 1.0, 0.0) for k in range(2)
            ]
            unpack[pl.ds(pl.multiple_of(i * pair, pair), pair), :] = jnp.concatenate(made, axis=0).astype(BF)
            return 0

        lax.fori_loop(0, EP // 2, body, 0, unroll=4)
        unpack_t[...] = unpack[...].T

    def build_factor():
        step = min(LANES, rows)

        def body(i, _):
            at = pl.ds(pl.multiple_of(i * step, step), step)
            wanted = 2 * (lax.broadcasted_iota(jnp.int32, (step, 1), 0) + i * step) + c
            found = jnp.where(positions == wanted, rw[...], 0.0)
            factor[at, :] = jnp.broadcast_to(jnp.sum(found, axis=1, keepdims=True), (step, LANES))
            return 0

        lax.fori_loop(0, rows // step, body, 0)

    build_place(0)
    tok_copy.wait()
    for copy in small[1:]:
        copy.wait()
    squares = jnp.zeros((tok_v.shape[0], 1), F32)
    for part_at in range(0, model, 512):
        some = tok_v[:, pl.ds(part_at, 512)].astype(F32)
        squares = squares + jnp.sum(some * some, axis=-1, keepdims=True)
    scale = lax.rsqrt(squares / model + 1e-06)
    normed = []
    for ahead in (0, FAR):
        columns = pl.ds(pl.multiple_of(wrap(y + ahead) * width, width), width)
        normed.append((tok_v[:, columns].astype(F32) * scale * gain[:, columns]).astype(BF))

    def pack(some, q):
        packed = jnp.dot(place[pl.ds(0, half_slots), :], some, preferred_element_type=F32)
        for h in range(2):
            sendbuf[q + h] = packed[:, h * LANES:(h + 1) * LANES].astype(BF).reshape(EP, slots, LANES)

    def exchange(q):
        def body(i, _):
            other = peer(i)
            remote(
                sendbuf.at[q, other], recvbuf.at[q, block], ep_send.at[q], ep_recv.at[q], chip(other, c)
            ).start()
            return 0

        lax.fori_loop(1, EP, body, 0)
        COPY(sendbuf.at[q, block], recvbuf.at[q, block], ep_recv.at[q]).start()

    pack(normed[0], 0)
    pl.semaphore_wait(barrier, plane - 1 + 2)
    exchange(0)
    exchange(1)
    pack(normed[1], 2)

    sibling = (z, x, y, 1 - c)
    shared = [
        remote(gate, gu_v.at[:, pl.ds(2 * ff, ff)], wx_send.at[0], wx_recv.at[0], sibling),
        remote(up, gu_v.at[:, pl.ds(3 * ff, ff)], wx_send.at[1], wx_recv.at[1], sibling),
        remote(down, dw_v.at[pl.ds(ff, ff), :], wx_send.at[2], wx_recv.at[2], sibling),
    ]
    for copy in shared:
        copy.start()
    exchange(2)
    exchange(3)
    build_unpack()

    def ag_copy(way, u, h):
        source = wrap(y + ((0, -1, FAR) if way == 0 else (0, 1, FAR))[u])
        where = ag.at[h, source]
        return remote(where, where, ag_send.at[way, u, h], ag_recv.at[way, u, h], along(way))

    def compact(q):
        COPY(recvbuf.at[q], recvbuf.at[q], ep_recv.at[q]).wait()
        u, h = q // 2, q % 2
        ag[h, wrap(y + u * FAR)] = jnp.dot(
            unpack_t[...], recvbuf[q].reshape(half_slots, LANES), preferred_element_type=F32
        ).astype(BF)
        for way in range(2):
            ag_copy(way, 2 * u, h).start()

    def gather_in(parts, begin=False):
        x_rows = jnp.concatenate([ag[h, source] for h, source in parts], axis=1)

        def tile(n, _):
            n_at = pl.ds(pl.multiple_of(n * ff, ff), ff)
            weight = jnp.concatenate(
                [gu_v[pl.ds(pl.multiple_of(source * width + h * LANES, LANES), LANES), n_at] for h, source in parts],
                axis=0,
            )
            product = jnp.dot(x_rows, weight, preferred_element_type=F32)
            if begin:
                acc[:, n_at] = product
            else:
                acc[:, n_at] += product
            return 0

        lax.fori_loop(0, 4, tile, 0)

    def whole(offset):
        source = wrap(y + offset)
        return [(0, source), (1, source)]

    compact(0)
    build_factor()
    build_place(1)
    place_t[...] = place[...].T
    compact(1)
    for copy in own:
        copy.wait()
    for copy in shared[:2]:
        copy.wait_recv()
    gather_in(whole(0), True)
    for h in range(2):
        for way in range(2):
            ag_copy(way, 0, h).wait_recv()
            ag_copy(way, 1, h).start()
    for offset in (-1, 1):
        gather_in(whole(offset))
    for q in (2, 3):
        compact(q)
    gather_in(whole(FAR))
    for way in range(2):
        for h in range(2):
            ag_copy(way, 1, h).wait_recv()
        gather_in(whole((-2, 2)[way]))
    for h in range(2):
        for way in range(2):
            ag_copy(way, 2, h).wait_recv()
        gather_in([(h, wrap(y - 1 + FAR)), (h, wrap(y + 1 + FAR))])

    for s in range(2):
        gate_pre = acc[:, pl.ds(2 * s * ff, ff)]
        up_pre = acc[:, pl.ds((2 * s + 1) * ff, ff)]
        hidden[:, pl.ds(s * ff, ff)] = (gate_pre / (1.0 + jnp.exp(-gate_pre)) * up_pre).astype(BF)
    shared[2].wait_recv()

    def terms(offset):
        target = wrap(y + offset)
        part[offset % NY] = jnp.dot(
            hidden[...], dw_v[:, pl.ds(pl.multiple_of(target * width, width), width)],
            preferred_element_type=F32,
        )

    piece = [pl.ds(0, rows // 2), pl.ds(rows // 2, rows // 2)]

    def rs_copy(way, h, hop, s):
        source = rs_first.at[way, h] if hop == 0 else rs.at[way, h, hop - 1, piece[s]]
        return remote(
            source, rs.at[way, h, hop, piece[s]],
            rs_send.at[way, h, hop, s], rs_recv.at[way, h, hop, s], along(way),
        )

    def pass_on(way, h, hop, s):
        ahead = FAR - hop if way == 0 else hop - FAR
        mine = part[ahead % NY, piece[s], pl.ds(h * LANES, LANES)]
        if hop == 0:
            rs_first[way, h] = mine.astype(BF)
        else:
            if hop > 1 or s == way:
                rs_copy(way, h, hop - 1, s).wait_recv()
                mine = mine + rs[way, h, hop - 1, piece[s]].astype(F32)
            rs[way, h, hop - 1, piece[s]] = mine.astype(BF)
        rs_copy(way, h, hop, s).start()

    def each_way(h, hop, chained):
        for way in range(2):
            pass_on(way, h, hop, way if chained else 1 - way)

    def finish(h):
        for way in range(2):
            for s in range(2):
                rs_copy(way, h, FAR - 1, s).wait_recv()
        total = part[0, :, pl.ds(h * LANES, LANES)]
        for way in range(2):
            total = total + rs[way, h, FAR - 1].astype(F32)
        weighted = (total * factor[...]).astype(BF)
        back[h] = (
            jnp.dot(unpack[...], weighted, preferred_element_type=F32).astype(BF).reshape(EP, slots, LANES)
        )
        rel = lax.rem(c + h, 2)

        def give(i, _):
            other = peer(i)
            remote(back.at[h, other], ret.at[rel, block], ret_send, ret_recv, chip(other, h)).start()
            return 0

        lax.fori_loop(1, EP, give, 0)

        @pl.when(c == h)
        def _():
            COPY(back.at[h, block], ret.at[rel, block], ret_recv).start()

        @pl.when(c != h)
        def _():
            remote(back.at[h, block], ret.at[rel, block], ret_send, ret_recv, chip(block, h)).start()

    terms(FAR)
    for h in range(2):
        each_way(h, 0, True)
    for offset in (FAR - 1, 1 - FAR):
        terms(offset)
    for h in range(2):
        each_way(h, 1, False)
    for hop in range(2, FAR):
        for offset in (FAR - hop, hop - FAR):
            terms(offset)
    terms(0)
    for h in range(2):
        each_way(h, 1, True)
    for hop in range(2, FAR):
        for h in range(2):
            for chained in (False, True):
                each_way(h, hop, chained)
    for h in range(2):
        finish(h)

    COPY(ret, ret, ret_recv).wait()
    out[...] = jnp.dot(
        place_t[...], ret[...].reshape(2 * half_slots, LANES), preferred_element_type=F32
    ).astype(BF)

    for q in range(4):
        sent = sendbuf.at[q, pl.ds(0, EP - 1)]
        COPY(sent, sent, ep_send.at[q]).wait()
    for h in range(2):
        for way in range(2):
            for u in range(3):
                ag_copy(way, u, h).wait_send()
            for hop in range(FAR):
                for s in range(2):
                    if hop > 0 or s == way:
                        rs_copy(way, h, hop, s).wait_send()
    for copy in shared:
        copy.wait_send()
    for h in range(2):
        sent = back.at[h, pl.ds(0, EP - h)]
        COPY(sent, sent, ret_send).wait()


def shards(tokens, norm_gain, chosen, route_weight, gate_weight, up_weight, down_weight):
    tok_rows, model = tokens.shape
    experts, capacity = chosen.shape
    ff = gate_weight.shape[2]
    slots = 3 * tok_rows // 32
    rows = capacity // 2
    vmem = pl.BlockSpec(memory_space=pltpu.VMEM)
    hbm = pl.BlockSpec(memory_space=pl.ANY)
    dma = pltpu.SemaphoreType.DMA
    return pl.pallas_call(
        functools.partial(kernel, slots),
        out_shape=jax.ShapeDtypeStruct((tok_rows, model // (NY * NC)), BF),
        in_specs=[hbm] * 7,
        out_specs=vmem,
        scratch_shapes=[
            pltpu.VMEM((tok_rows, model), BF),
            pltpu.VMEM((1, model), F32),
            pltpu.VMEM((experts, capacity), jnp.int32),
            pltpu.VMEM((1, capacity), F32),
            pltpu.VMEM((model, 4 * ff), BF),
            pltpu.VMEM((2 * ff, model), BF),
            pltpu.VMEM((experts, capacity), F32),
            pltpu.VMEM((experts, capacity), jnp.int32),
            pltpu.VMEM((EP, rows), jnp.int32),
            pltpu.VMEM((rows, LANES), F32),
            pltpu.VMEM((2 * EP * slots, tok_rows), BF),
            pltpu.VMEM((tok_rows, 2 * EP * slots), BF),
            pltpu.VMEM((EP * slots, rows), BF),
            pltpu.VMEM((rows, EP * slots), BF),
            pltpu.VMEM((4, EP, slots, LANES), BF),
            pltpu.VMEM((4, EP, slots, LANES), BF),
            pltpu.VMEM((2, NY, rows, LANES), BF),
            pltpu.VMEM((rows, 4 * ff), F32),
            pltpu.VMEM((rows, 2 * ff), BF),
            pltpu.VMEM((NY, rows, 2 * LANES), F32),
            pltpu.VMEM((2, 2, rows // 2, LANES), BF),
            pltpu.VMEM((2, 2, FAR, rows, LANES), BF),
            pltpu.VMEM((2, EP, slots, LANES), BF),
            pltpu.VMEM((2, EP, slots, LANES), BF),
            dma(()),
            dma((3,)),
            dma((3,)),
            dma((3,)),
            dma((3,)),
            dma((4,)),
            dma((4,)),
            dma((2, 3, 2)),
            dma((2, 3, 2)),
            dma((2, 2, FAR, 2)),
            dma((2, 2, FAR, 2)),
            dma(()),
            dma(()),
        ],
        compiler_params=pltpu.CompilerParams(
            collective_id=0, has_side_effects=True, vmem_limit_bytes=56 * 1024 * 1024
        ),
    )(tokens, norm_gain.reshape(1, -1), chosen, route_weight, gate_weight[0], up_weight[0], down_weight[0])


def solution(mesh):
    finer = Mesh(mesh.devices.reshape(NZ, NX, NY, NC), ("z", "x", "y", "c"))
    ep, tp = ("z", "x"), ("y", "c")
    in_specs = (
        P(ep, None),
        P(),
        P(),
        P(ep, None),
        P(ep, None, tp),
        P(ep, None, tp),
        P(ep, tp, None),
    )
    return jax.shard_map(
        shards, mesh=finer, in_specs=in_specs, out_specs=P(ep, tp), check_vma=False
    )
```

time: 86.6 us -> 81.3 us (0.939)
  Pallas kernels: 84.9 us -> 79.7 us
    pallas_call x1, Pallas kernels: 84.9 us -> 79.7 us  [shards(): pl.pallas_call(functools.partial(kernel, slots), out_shape=jax.ShapeDtype...]
where the time goes in v3:
time: 81.3 us; the launch traced here: 81.2 us
  Pallas kernels  79.7 us (98%)
  local copies, waits for them, and re-layouts  1.47 us (2%)
    pallas_call x1, Pallas kernels, shards(): pl.pallas_call(functools.partial(kernel, slots), out_shape=jax.ShapeDtype...  79.7 us

profile of v3, /device:TPU:1, one launch (start us, length us, event | category | flops | bytes accessed | tf_op | source)
XLA Modules:
  0.0 81.2 jit_solution(18277396361728061725)
XLA Ops:
  0.0 79.7 %shard_map.73 = bf16[256,128]{1,0:T(8,128)(2,1)} custom-call(bf16[256,2048]{1,0:T(8,128)(2,1)} %tokens.1, f32[1,2048]{1,0:T(1,128)} %bitcast.7, s32[32,1024]{1,0:T(8,128)} %chosen_in.1, f32[1,1024]{1,0:T(1,128)} %rw_in.1, bf16[2048,256]{1,0:T(8,128)(2,1)} %bitcast.4, bf16[2048,256]{1,0:T(8,128)(2,1)} %bitcast.5, bf16[256,2048]{1,0:T(8,128)(2,1)} %bitcast.6), custom_call_target="tpu_custom_call" | custom-call | tf_op jit(solution)/shard_map/pallas_call | solution.py:386
  79.7 1.5 %copy.9 = bf16[256,128]{1,0:T(8,128)(2,1)} copy(bf16[256,128]{1,0:T(8,128)(2,1)} %shard_map.73) | data formatting | bytes 131072

commit v4 on v3

--- a/solution.py
+++ b/solution.py
@@ -68,26 +68,23 @@
         copy.start()
 
     def peer(i):
-        k, r = (i - 1) // NX, lax.rem(i - 1, NX)
-        away = NZ // 2 - (k + 1) // 2
-        dz = jnp.where(lax.rem(k, 2) == 0, NZ - away, away)
-        return lax.rem(z + dz, NZ) * NX + lax.rem(x + NX - 1 - r, NX)
+        step = (i + 1) // 2
+        return lax.rem(block + jnp.where(lax.rem(i, 2) == 1, step, EP - step), EP)
 
     barrier = pltpu.get_barrier_semaphore()
     plane = EP * NC
-    me = block * NC + c
-
-    def greet(i, _):
-        other = lax.rem(me + i, plane)
-        pl.semaphore_signal(
-            barrier, inc=1, device_id=chip(other // NC, lax.rem(other, NC)),
-            device_id_type=pl.DeviceIdType.MESH,
-        )
-        return 0
-
+    apart = sorted(range(NZ), key=lambda dz: -min(dz, NZ - dz))
+    for dz in apart:
+        for dx in range(NX - 1, -1, -1):
+            for dc in range(NC):
+                if dz or dx or dc:
+                    pl.semaphore_signal(
+                        barrier, inc=1,
+                        device_id=(lax.rem(z + dz, NZ), lax.rem(x + dx, NX), y, lax.rem(c + dc, NC)),
+                        device_id_type=pl.DeviceIdType.MESH,
+                    )
     for way in range(2):
         pl.semaphore_signal(barrier, inc=1, device_id=along(way), device_id_type=pl.DeviceIdType.MESH)
-    lax.fori_loop(1, plane, greet, 0)
 
     tok_rows, capacity = tok_v.shape[0], chosen.shape[1]
     first = block * tok_rows
@@ -162,14 +159,13 @@
         some = tok_v[:, pl.ds(part_at, 512)].astype(F32)
         squares = squares + jnp.sum(some * some, axis=-1, keepdims=True)
     scale = lax.rsqrt(squares / model + 1e-06)
-    normed = []
-    for ahead in (0, FAR):
-        columns = pl.ds(pl.multiple_of(wrap(y + ahead) * width, width), width)
-        normed.append((tok_v[:, columns].astype(F32) * scale * gain[:, columns]).astype(BF))
+    def normed(start, size):
+        columns = pl.ds(pl.multiple_of(start, LANES), size)
+        return (tok_v[:, columns].astype(F32) * scale * gain[:, columns]).astype(BF)
 
     def pack(some, q):
         packed = jnp.dot(place[pl.ds(0, half_slots), :], some, preferred_element_type=F32)
-        for h in range(2):
+        for h in range(some.shape[1] // LANES):
             sendbuf[q + h] = packed[:, h * LANES:(h + 1) * LANES].astype(BF).reshape(EP, slots, LANES)
 
     def exchange(q):
@@ -183,11 +179,11 @@
         lax.fori_loop(1, EP, body, 0)
         COPY(sendbuf.at[q, block], recvbuf.at[q, block], ep_recv.at[q]).start()
 
-    pack(normed[0], 0)
+    pack(normed(y * width, width), 0)
     pl.semaphore_wait(barrier, plane - 1 + 2)
     exchange(0)
     exchange(1)
-    pack(normed[1], 2)
+    pack(normed(wrap(y + FAR) * width, width), 2)
 
     sibling = (z, x, y, 1 - c)
     shared = [
@@ -197,8 +193,8 @@
     ]
     for copy in shared:
         copy.start()
-    exchange(2)
-    exchange(3)
+    for q in range(2, 4):
+        exchange(q)
     build_unpack()
 
     def ag_copy(way, u, h):
@@ -351,11 +347,6 @@
     for h in range(2):
         finish(h)
 
-    COPY(ret, ret, ret_recv).wait()
-    out[...] = jnp.dot(
-        place_t[...], ret[...].reshape(2 * half_slots, LANES), preferred_element_type=F32
-    ).astype(BF)
-
     for q in range(4):
         sent = sendbuf.at[q, pl.ds(0, EP - 1)]
         COPY(sent, sent, ep_send.at[q]).wait()
@@ -369,6 +360,10 @@
                         rs_copy(way, h, hop, s).wait_send()
     for copy in shared:
         copy.wait_send()
+    COPY(ret, ret, ret_recv).wait()
+    out[...] = jnp.dot(
+        place_t[...], ret[...].reshape(2 * half_slots, LANES), preferred_element_type=F32
+    ).astype(BF)
     for h in range(2):
         sent = back.at[h, pl.ds(0, EP - h)]
         COPY(sent, sent, ret_send).wait()
@@ -385,7 +380,7 @@
     dma = pltpu.SemaphoreType.DMA
     return pl.pallas_call(
         functools.partial(kernel, slots),
-        out_shape=jax.ShapeDtypeStruct((tok_rows, model // (NY * NC)), BF),
+        out_shape=pltpu.VMEM((tok_rows, model // (NY * NC)), BF),
         in_specs=[hbm] * 7,
         out_specs=vmem,
         scratch_shapes=[

time: 81.3 us -> 76.4 us (0.940)
  Pallas kernels: 79.7 us -> 75.7 us
  local copies, waits for them, and re-layouts: 1.47 us -> 0.63 us
    pallas_call x1, Pallas kernels: 79.7 us -> 75.7 us  [shards(): pl.pallas_call(functools.partial(kernel, slots), out_shape=pltpu.VMEM((to...]
    unnamed x1, local copies, waits for them, and re-layouts: 1.47 us -> 0.63 us
where the time goes in v4:
time: 76.4 us; the launch traced here: 76.3 us
  Pallas kernels  75.7 us (99%)
    pallas_call x1, Pallas kernels, shards(): pl.pallas_call(functools.partial(kernel, slots), out_shape=pltpu.VMEM((to...  75.7 us

profile of v4, /device:TPU:1, one launch (start us, length us, event | category | flops | bytes accessed | tf_op | source)
XLA Modules:
  0.0 76.3 jit_solution(5944386795744018025)
XLA Ops:
  0.0 75.7 %shard_map.73 = bf16[256,128]{1,0:T(8,128)(2,1)S(1)} custom-call(bf16[256,2048]{1,0:T(8,128)(2,1)} %tokens.1, f32[1,2048]{1,0:T(1,128)} %bitcast.7, s32[32,1024]{1,0:T(8,128)} %chosen_in.1, f32[1,1024]{1,0:T(1,128)} %rw_in.1, bf16[2048,256]{1,0:T(8,128)(2,1)} %bitcast.4, bf16[2048,256]{1,0:T(8,128)(2,1)} %bitcast.5, bf16[256,2048]{1,0:T(8,128)(2,1)} %bitcast.6), custom_call_target="tpu_custom_call" | custom-call | tf_op jit(solution)/shard_map/pallas_call | solution.py:381
  75.7 0.6 copy.9

commit v5 on v4

--- a/solution.py
+++ b/solution.py
@@ -197,10 +197,17 @@
         exchange(q)
     build_unpack()
 
-    def ag_copy(way, u, h):
+    piece = [pl.ds(0, rows // 2), pl.ds(rows // 2, rows // 2)]
+
+    def ag_copy(way, u, h, s=None):
         source = wrap(y + ((0, -1, FAR) if way == 0 else (0, 1, FAR))[u])
-        where = ag.at[h, source]
-        return remote(where, where, ag_send.at[way, u, h], ag_recv.at[way, u, h], along(way))
+        where = ag.at[h, source] if s is None else ag.at[h, source, piece[s]]
+        at = (way, u, h, 0 if s is None else s)
+        return remote(where, where, ag_send.at[at], ag_recv.at[at], along(way))
+
+    def send_on(u, h, s=None):
+        for way in range(2):
+            ag_copy(way, u, h, s).start()
 
     def compact(q):
         COPY(recvbuf.at[q], recvbuf.at[q], ep_recv.at[q]).wait()
@@ -208,11 +215,9 @@
         ag[h, wrap(y + u * FAR)] = jnp.dot(
             unpack_t[...], recvbuf[q].reshape(half_slots, LANES), preferred_element_type=F32
         ).astype(BF)
-        for way in range(2):
-            ag_copy(way, 2 * u, h).start()
-
-    def gather_in(parts, begin=False):
-        x_rows = jnp.concatenate([ag[h, source] for h, source in parts], axis=1)
+
+    def gather_in(parts, begin=False, r_at=pl.ds(0, rows)):
+        x_rows = jnp.concatenate([ag[h, source, r_at] for h, source in parts], axis=1)
 
         def tile(n, _):
             n_at = pl.ds(pl.multiple_of(n * ff, ff), ff)
@@ -222,9 +227,9 @@
             )
             product = jnp.dot(x_rows, weight, preferred_element_type=F32)
             if begin:
-                acc[:, n_at] = product
+                acc[r_at, n_at] = product
             else:
-                acc[:, n_at] += product
+                acc[r_at, n_at] += product
             return 0
 
         lax.fori_loop(0, 4, tile, 0)
@@ -234,10 +239,12 @@
         return [(0, source), (1, source)]
 
     compact(0)
+    send_on(0, 0)
     build_factor()
     build_place(1)
     place_t[...] = place[...].T
     compact(1)
+    send_on(0, 1)
     for copy in own:
         copy.wait()
     for copy in shared[:2]:
@@ -249,32 +256,33 @@
             ag_copy(way, 1, h).start()
     for offset in (-1, 1):
         gather_in(whole(offset))
-    for q in (2, 3):
-        compact(q)
+    compact(2)
+    send_on(2, 0, 0)
+    compact(3)
+    for h, s in ((1, 0), (0, 1), (1, 1)):
+        send_on(2, h, s)
     gather_in(whole(FAR))
     for way in range(2):
         for h in range(2):
             ag_copy(way, 1, h).wait_recv()
         gather_in(whole((-2, 2)[way]))
-    for h in range(2):
-        for way in range(2):
-            ag_copy(way, 2, h).wait_recv()
-        gather_in([(h, wrap(y - 1 + FAR)), (h, wrap(y + 1 + FAR))])
-
-    for s in range(2):
-        gate_pre = acc[:, pl.ds(2 * s * ff, ff)]
-        up_pre = acc[:, pl.ds((2 * s + 1) * ff, ff)]
-        hidden[:, pl.ds(s * ff, ff)] = (gate_pre / (1.0 + jnp.exp(-gate_pre)) * up_pre).astype(BF)
-    shared[2].wait_recv()
-
-    def terms(offset):
+
+    def rest(s):
+        for h in range(2):
+            for way in range(2):
+                ag_copy(way, 2, h, s).wait_recv()
+            gather_in([(h, wrap(y - 1 + FAR)), (h, wrap(y + 1 + FAR))], r_at=piece[s])
+        for n in range(2):
+            gate_pre = acc[piece[s], pl.ds(2 * n * ff, ff)]
+            up_pre = acc[piece[s], pl.ds((2 * n + 1) * ff, ff)]
+            hidden[piece[s], pl.ds(n * ff, ff)] = (gate_pre / (1.0 + jnp.exp(-gate_pre)) * up_pre).astype(BF)
+
+    def terms(offset, s):
         target = wrap(y + offset)
-        part[offset % NY] = jnp.dot(
-            hidden[...], dw_v[:, pl.ds(pl.multiple_of(target * width, width), width)],
+        part[offset % NY, piece[s]] = jnp.dot(
+            hidden[piece[s], :], dw_v[:, pl.ds(pl.multiple_of(target * width, width), width)],
             preferred_element_type=F32,
         )
-
-    piece = [pl.ds(0, rows // 2), pl.ds(rows // 2, rows // 2)]
 
     def rs_copy(way, h, hop, s):
         source = rs_first.at[way, h] if hop == 0 else rs.at[way, h, hop - 1, piece[s]]
@@ -327,19 +335,27 @@
         def _():
             remote(back.at[h, block], ret.at[rel, block], ret_send, ret_recv, chip(block, h)).start()
 
-    terms(FAR)
-    for h in range(2):
-        each_way(h, 0, True)
-    for offset in (FAR - 1, 1 - FAR):
-        terms(offset)
-    for h in range(2):
-        each_way(h, 1, False)
-    for hop in range(2, FAR):
-        for offset in (FAR - hop, hop - FAR):
-            terms(offset)
-    terms(0)
+    for s in range(2):
+        rest(s)
+        if s == 0:
+            shared[2].wait_recv()
+        terms(FAR, s)
+        for h in range(2):
+            pass_on(s, h, 0, s)
+        near = 1 - FAR if s == 0 else FAR - 1
+        terms(near, s)
+        for h in range(2):
+            pass_on(1 - s, h, 1, s)
+    terms(FAR - 1, 0)
+    terms(1 - FAR, 1)
+    for s in range(2):
+        for hop in range(2, FAR):
+            for offset in (FAR - hop, hop - FAR):
+                terms(offset, s)
     for h in range(2):
         each_way(h, 1, True)
+    for s in range(2):
+        terms(0, s)
     for hop in range(2, FAR):
         for h in range(2):
             for chained in (False, True):
@@ -352,8 +368,10 @@
         COPY(sent, sent, ep_send.at[q]).wait()
     for h in range(2):
         for way in range(2):
-            for u in range(3):
+            for u in range(2):
                 ag_copy(way, u, h).wait_send()
+            for s in range(2):
+                ag_copy(way, 2, h, s).wait_send()
             for hop in range(FAR):
                 for s in range(2):
                     if hop > 0 or s == way:
@@ -415,8 +433,8 @@
             dma((3,)),
             dma((4,)),
             dma((4,)),
-            dma((2, 3, 2)),
-            dma((2, 3, 2)),
+            dma((2, 3, 2, 2)),
+            dma((2, 3, 2, 2)),
             dma((2, 2, FAR, 2)),
             dma((2, 2, FAR, 2)),
             dma(()),

time: 76.4 us -> 75.4 us (0.987)
  Pallas kernels: 75.7 us -> 74.7 us
    pallas_call x1, Pallas kernels: 75.7 us -> 74.7 us  [shards(): pl.pallas_call(functools.partial(kernel, slots), out_shape=pltpu.VMEM((to...]
where the time goes in v5:
time: 75.4 us; the launch traced here: 75.3 us
  Pallas kernels  74.7 us (99%)
    pallas_call x1, Pallas kernels, shards(): pl.pallas_call(functools.partial(kernel, slots), out_shape=pltpu.VMEM((to...  74.7 us

profile of v5, /device:TPU:1, one launch (start us, length us, event | category | flops | bytes accessed | tf_op | source)
XLA Modules:
  0.0 75.3 jit_solution(2322138855550505175)
XLA Ops:
  0.0 74.7 %shard_map.73 = bf16[256,128]{1,0:T(8,128)(2,1)S(1)} custom-call(bf16[256,2048]{1,0:T(8,128)(2,1)} %tokens.1, f32[1,2048]{1,0:T(1,128)} %bitcast.7, s32[32,1024]{1,0:T(8,128)} %chosen_in.1, f32[1,1024]{1,0:T(1,128)} %rw_in.1, bf16[2048,256]{1,0:T(8,128)(2,1)} %bitcast.4, bf16[2048,256]{1,0:T(8,128)(2,1)} %bitcast.5, bf16[256,2048]{1,0:T(8,128)(2,1)} %bitcast.6), custom_call_target="tpu_custom_call" | custom-call | tf_op jit(solution)/shard_map/pallas_call | solution.py:399
  74.7 0.6 copy.9

commit v6 on v5

--- a/solution.py
+++ b/solution.py
@@ -181,10 +181,6 @@
 
     pack(normed(y * width, width), 0)
     pl.semaphore_wait(barrier, plane - 1 + 2)
-    exchange(0)
-    exchange(1)
-    pack(normed(wrap(y + FAR) * width, width), 2)
-
     sibling = (z, x, y, 1 - c)
     shared = [
         remote(gate, gu_v.at[:, pl.ds(2 * ff, ff)], wx_send.at[0], wx_recv.at[0], sibling),
@@ -193,6 +189,10 @@
     ]
     for copy in shared:
         copy.start()
+    exchange(0)
+    exchange(1)
+    pack(normed(wrap(y + FAR) * width, width), 2)
+
     for q in range(2, 4):
         exchange(q)
     build_unpack()
@@ -245,15 +245,16 @@
     place_t[...] = place[...].T
     compact(1)
     send_on(0, 1)
-    for copy in own:
-        copy.wait()
-    for copy in shared[:2]:
-        copy.wait_recv()
-    gather_in(whole(0), True)
     for h in range(2):
         for way in range(2):
             ag_copy(way, 0, h).wait_recv()
             ag_copy(way, 1, h).start()
+        if h == 0:
+            for copy in own:
+                copy.wait()
+            for copy in shared[:2]:
+                copy.wait_recv()
+            gather_in(whole(0), True)
     for offset in (-1, 1):
         gather_in(whole(offset))
     compact(2)

time: 75.4 us -> 75.2 us (level)
  no operation moved by 1% of the time
where the time goes in v6:
time: 75.2 us; the launch traced here: 75.1 us
  Pallas kernels  74.4 us (99%)
    pallas_call x1, Pallas kernels, shards(): pl.pallas_call(functools.partial(kernel, slots), out_shape=pltpu.VMEM((to...  74.4 us

profile of v6, /device:TPU:1, one launch (start us, length us, event | category | flops | bytes accessed | tf_op | source)
XLA Modules:
  0.0 75.1 jit_solution(16776414052856932349)
XLA Ops:
  0.0 74.4 %shard_map.73 = bf16[256,128]{1,0:T(8,128)(2,1)S(1)} custom-call(bf16[256,2048]{1,0:T(8,128)(2,1)} %tokens.1, f32[1,2048]{1,0:T(1,128)} %bitcast.7, s32[32,1024]{1,0:T(8,128)} %chosen_in.1, f32[1,1024]{1,0:T(1,128)} %rw_in.1, bf16[2048,256]{1,0:T(8,128)(2,1)} %bitcast.4, bf16[2048,256]{1,0:T(8,128)(2,1)} %bitcast.5, bf16[256,2048]{1,0:T(8,128)(2,1)} %bitcast.6), custom_call_target="tpu_custom_call" | custom-call | tf_op jit(solution)/shard_map/pallas_call | solution.py:400
  74.4 0.6 copy.9
